TPU v7x, 512 devices: a 4x2x32 block of a 4x8x32 slice. The times are simulated.
512 devices in a mesh: grp: 2 (over y), sp: 32 (over z), tp: 8 (over x, core).
Axes of the slice: x: 4, y: 2, z: 32, core: 2. Of those that a mesh axis runs over, the one named last changes fastest.
The devices are a block of a 4x8x32 slice.
Arguments:
- latent: bfloat16 [24576, 2048], P(('grp', 'sp')), parts along dimension 0, may hold values from -6 to 6
- conditioning: bfloat16 [4096], P(('grp', 'sp')), parts along dimension 0, may hold values from -6 to 6
- context: bfloat16 [1024, 2048], P(('grp', 'sp')), parts along dimension 0, may hold values from -6 to 6
- ctx_vector: bfloat16 [2048], P('sp'), may hold values from -6 to 6
- w_shift: bfloat16 [2048, 2048], P('sp', 'tp'), may hold values from -0.25 to 0.25
- w_scale: bfloat16 [2048, 2048], P('sp', 'tp'), may hold values from -0.25 to 0.25
- w_gate: bfloat16 [2048, 2048], P('sp', 'tp'), may hold values from -0.25 to 0.25
- norm_gain: bfloat16 [2048], replicated, may hold values from 0.099609375 to 1.8984375
- w_query: bfloat16 [2048, 1024], P(None, 'tp'), may hold values from -1 to 1
- w_key: bfloat16 [2048, 1024], P(None, 'tp'), may hold values from -1 to 1
- w_value: bfloat16 [2048, 1024], P(None, 'tp'), may hold values from -0.125 to 0.125
- offset_bias: float32 [16, 15, 31], P('tp'), may hold values from 1.5 to 4.5
- w_out: bfloat16 [1024, 2048], P(None, 'tp'), may hold values from -0.75 to 0.75
Outputs:
- mixed_out: bfloat16 [24576, 2048], P(('grp', 'sp'), 'tp'), parts along dimension 0
There are 2 independent parts, one for each index of `grp`. A program takes and returns all parts, laid end to end along the dimension named above; an argument that names none is the same for every part. Nothing has to cross between parts.
All inputs are finite; a program needn't handle non-finite values.
Results may differ from a plain program's by a relative error of at most 0.011.
Values may be sent and summed in bfloat16 or wider, within the bound.
A program may use at most 64 MiB of HBM per device.

v0:
```python
import jax
import jax.numpy as jnp
from jax import lax
from jax.sharding import PartitionSpec as P

HEAD_DIM = 64
GRID_W = 64
WIN_H = 8
WIN_W = 16


EPSILON = 1e-06


def from_everyone(value, axis):
    copies = jnp.broadcast_to(value, (lax.axis_size(axis), *value.shape))
    return lax.all_to_all(copies, axis, split_axis=0, concat_axis=0, tiled=True)


def taken_together(value, axis):
    everything = from_everyone(value, axis)
    return jnp.sum(everything, axis=0)


def packed_total(arrays, axis):
    flat, at, done = (jnp.concatenate([a.reshape(-1) for a in arrays]), 0, [])
    total = taken_together(flat, axis)
    for a in arrays:
        done.append(total[at : at + a.size].reshape(a.shape))
        at += a.size
    return tuple(done)


def sent_together(arrays, axis, dim, along):
    both = jnp.concatenate(arrays, axis=along)
    filled, at, done = (lax.all_gather(both, axis, axis=dim, tiled=True), 0, [])
    for a in arrays:
        done.append(lax.slice_in_dim(filled, at, at + a.shape[along], axis=along))
        at += a.shape[along]
    return tuple(done)


def joined_along(blocks, dim):
    blocks = jnp.moveaxis(blocks, 0, dim)
    dims = blocks.shape
    return blocks.reshape(*dims[:dim], dims[dim] * dims[dim + 1], *dims[dim + 2 :])


def gathered_copies(value, axis, dim):
    return joined_along(from_everyone(value, axis), dim)


def extended(block, sides, width):
    for axis, dim in sides:
        count = lax.axis_size(axis)
        forward = [(i, i + 1) for i in range(count - 1)]
        backward = [(target, source) for source, target in forward]
        low = lax.ppermute(
            lax.slice_in_dim(block, block.shape[dim] - width, None, axis=dim), axis, forward
        )
        high = lax.ppermute(lax.slice_in_dim(block, 0, width, axis=dim), axis, backward)
        block = jnp.concatenate([low, block, high], axis=dim)
    return block


def modulated_norm(inputs, norm_gain, shift_vec, scale_vec):
    floats = inputs.astype(jnp.float32)
    inverse = lax.rsqrt(jnp.mean(floats * floats, axis=-1, keepdims=True) + EPSILON)
    return (
        floats * inverse * norm_gain.astype(jnp.float32) * (1.0 + scale_vec) + shift_vec
    ).astype(jnp.bfloat16)


def project(inputs, weight):
    return jnp.dot(inputs, weight, preferred_element_type=jnp.float32).astype(jnp.bfloat16)


def local(
    latent,
    conditioning,
    context,
    ctx_vector,
    w_shift,
    w_scale,
    w_gate,
    norm_gain,
    w_query,
    w_key,
    w_value,
    offset_bias,
    w_out,
):
    cols_tp = w_shift.shape[1]
    tp_index = lax.axis_index("tp")
    cond_act = jax.nn.silu(conditioning.astype(jnp.float32)).astype(jnp.bfloat16)
    ctx_act = jax.nn.silu(ctx_vector.astype(jnp.float32)).astype(jnp.bfloat16)
    both_acts = jnp.stack([cond_act, ctx_act])
    part_shift = jnp.dot(both_acts, w_shift, preferred_element_type=jnp.float32)
    part_scale = jnp.dot(both_acts, w_scale, preferred_element_type=jnp.float32)
    part_gate = jnp.dot(cond_act, w_gate, preferred_element_type=jnp.float32)
    shift_own, scale_own, gate_vec = packed_total((part_shift, part_scale, part_gate), "sp")
    shift_all, scale_all = sent_together((shift_own, scale_own), "tp", 1, 0)
    normed = modulated_norm(latent, norm_gain, shift_all[0], scale_all[0])
    queries = project(normed, w_query)
    keys_lat = project(normed, w_key)
    values_lat = project(normed, w_value)
    head_width = w_query.shape[1]
    local_heads = head_width // HEAD_DIM
    ctx_normed = modulated_norm(context, norm_gain, shift_all[1], scale_all[1])
    ctx_pairs = gathered_copies(
        jnp.concatenate([project(ctx_normed, w_key), project(ctx_normed, w_value)], axis=1), "sp", 0
    )
    ctx_keys = ctx_pairs[:, :head_width].reshape(-1, local_heads, HEAD_DIM)
    ctx_values = ctx_pairs[:, head_width:].reshape(-1, local_heads, HEAD_DIM)
    rows_dev = latent.shape[0] // GRID_W
    key_value = jnp.concatenate([keys_lat, values_lat], axis=1).reshape(
        rows_dev, GRID_W, 2 * head_width
    )
    padded = extended(key_value, (("sp", 0),), WIN_H // 2)
    grid_rows = rows_dev * lax.axis_size("sp")
    row_base = lax.axis_index("sp") * rows_dev
    global_rows = row_base + jnp.arange(rows_dev, dtype=jnp.int32)
    first_rows = jnp.clip(global_rows - WIN_H // 2, 0, grid_rows - WIN_H)
    starts = first_rows - row_base + WIN_H // 2
    windows = jax.vmap(
        lambda window_start: lax.dynamic_slice_in_dim(padded, window_start, WIN_H, 0)
    )(starts)
    key_window = windows[..., :head_width].reshape(rows_dev, WIN_H, GRID_W, local_heads, HEAD_DIM)
    value_window = windows[..., head_width:].reshape(rows_dev, WIN_H, GRID_W, local_heads, HEAD_DIM)
    query_grid = queries.reshape(rows_dev, GRID_W, local_heads, HEAD_DIM)
    scale_qk = HEAD_DIM ** (-0.5)
    columns = jnp.arange(GRID_W, dtype=jnp.int32)
    col_first = jnp.clip(columns - WIN_W // 2, 0, GRID_W - WIN_W)
    inside = (columns[None, :] >= col_first[:, None]) & (
        columns[None, :] < col_first[:, None] + WIN_W
    )
    col_offset = jnp.clip(columns[None, :] - columns[:, None] + WIN_W - 1, 0, 2 * WIN_W - 2)
    table_cols = offset_bias[:, :, col_offset]
    row_offsets = first_rows - global_rows + WIN_H - 1
    table_rows = jax.vmap(
        lambda offset_row: lax.dynamic_slice_in_dim(table_cols, offset_row, WIN_H, 1)
    )(row_offsets)
    win_scores = (
        jnp.einsum("rchd,rijhd->rhcij", query_grid, key_window, preferred_element_type=jnp.float32)
        * scale_qk
    )
    win_scores = jnp.where(
        inside[None, None, :, None, :], win_scores + table_rows.transpose(0, 1, 3, 2, 4), -jnp.inf
    )
    ctx_scores = (
        jnp.einsum("rchd,lhd->rhcl", query_grid, ctx_keys, preferred_element_type=jnp.float32)
        * scale_qk
    )
    highest = jnp.maximum(jnp.max(win_scores, axis=(3, 4)), jnp.max(ctx_scores, axis=3))
    win_exp = jnp.exp(win_scores - highest[..., None, None])
    ctx_exp = jnp.exp(ctx_scores - highest[..., None])
    totals = jnp.sum(win_exp, axis=(3, 4)) + jnp.sum(ctx_exp, axis=3)
    win_weights = (win_exp / totals[..., None, None]).astype(jnp.bfloat16)
    ctx_weights = (ctx_exp / totals[..., None]).astype(jnp.bfloat16)
    attended = jnp.einsum(
        "rhcij,rijhd->rchd", win_weights, value_window, preferred_element_type=jnp.float32
    )
    attended = attended + jnp.einsum(
        "rhcl,lhd->rchd", ctx_weights, ctx_values, preferred_element_type=jnp.float32
    )
    attended = attended.astype(jnp.bfloat16).reshape(rows_dev * GRID_W, head_width)
    branch = jnp.dot(gathered_copies(attended, "tp", 1), w_out, preferred_element_type=jnp.float32)
    residual = lax.dynamic_slice_in_dim(latent, tp_index * cols_tp, cols_tp, 1).astype(jnp.float32)
    return (residual + gate_vec * branch).astype(jnp.bfloat16)


def solution(mesh):
    return jax.shard_map(
        local,
        mesh=mesh,
        in_specs=(
            P(("grp", "sp"), None),
            P(("grp", "sp")),
            P(("grp", "sp"), None),
            P("sp"),
            P("sp", "tp"),
            P("sp", "tp"),
            P("sp", "tp"),
            P(),
            P(None, "tp"),
            P(None, "tp"),
            P(None, "tp"),
            P("tp", None, None),
            P(None, "tp"),
        ),
        out_specs=P(("grp", "sp"), "tp"),
        check_vma=False,
    )
```

profile of v0, /device:TPU:33, one launch (start us, length us, event | category | flops | bytes accessed | tf_op | source)
XLA Modules:
  0.0 197.7 jit_solution(8628353804982260367)
XLA Ops:
  4.2 46.3 %all-to-all-start = ((f32[32,1,1280]{2,1,0:T(1,128)}), f32[32,1,1280]{2,1,0:T(1,128)S(1)}, u32[]{:S(2)}, u32[]{:S(2)}) async-start(f32[32,1,1280]{2,1,0:T(1,128)} %broadcast_in_dim.14), calls=%async_computation | async-start | bytes 327680 | tf_op jit(solution)/shard_map/all_to_all | solution.py:17
  51.4 28.4 %gather_fusion.1 = f32[4096,2,15]{2,1,0:T(2,128)} fusion(f32[2,15,31]{1,0,2:T(2,128)S(1)} %copy.107, s32[4096]{0:T(1024)S(1)} %broadcast_clamp_fusion), kind=kCustom, calls=%fused_computation.1 | custom fusion | bytes 999424 | tf_op jit(solution)/shard_map/gather | solution.py:138
  79.8 5.4 %copy.108 = f32[64,64,2,15]{1,0,2,3:T(8,128)S(1)} copy(f32[64,64,2,15]{3,2,1,0:T(2,128)} %bitcast.100) | data formatting | bytes 983040 | tf_op jit(solution)/shard_map/gather | solution.py:138
  85.3 2.5 %gather_fusion.2 = f32[6,2,8,64,64]{4,3,1,2,0:T(8,128)} fusion(f32[2,15,64,64]{3,2,0,1:T(8,128)S(1)} %bitcast.96, s32[6]{0:T(128)S(1)} %shift-left_bitcast_fusion), kind=kCustom, calls=%fused_computation.2 | custom fusion | bytes 3145824 | tf_op jit(solution)/shard_map/vmap()/gather | solution.py:141
  87.8 3.7 %copy.109 = f32[6,2,8,64,64]{3,4,2,1,0:T(8,128)} copy(f32[6,2,8,64,64]{4,3,1,2,0:T(8,128)} %gather_fusion.2) | data formatting | bytes 3145728 | tf_op jit(solution)/shard_map/vmap()/gather | solution.py:141
  92.3 14.3 %all_gather.3 = f32[4,2048]{1,0:T(4,128)S(1)} all-gather(f32[4,256]{1,0:T(4,128)S(1)} %pad_maximum_fusion.4), channel_id=1, replica_groups=mesh['grp'=2,'sp'=32,'tp'=8] {'tp'}, dimensions={1}, use_global_device_ids=true | all-gather | bytes 36864 | tf_op jit(solution)/shard_map/all_gather | solution.py:36
  107.9 21.7 %all-to-all-start.1 = ((bf16[32,16,256]{2,1,0:T(8,128)(2,1)}), bf16[32,16,256]{2,1,0:T(8,128)(2,1)S(1)}, u32[]{:S(2)}, u32[]{:S(2)}) async-start(bf16[32,16,256]{2,1,0:T(8,128)(2,1)} %broadcast_in_dim.17), calls=%async_computation.1 | async-start | bytes 524288 | tf_op jit(solution)/shard_map/all_to_all | solution.py:17
  129.6 2.1 %fusion.4 = bf16[384,2048]{1,0:T(8,128)(2,1)S(1)} fusion(bf16[384,2048]{1,0:T(8,128)(2,1)} %param.13, f32[2048]{0:T(1024)S(1)} %bitcast.114, f32[2048]{0:T(1024)S(1)} %bitcast.115, f32[2048]{0:T(1024)S(1)} %convert_element_type.64, f32[384]{0:T(512)S(1)} %add_rsqrt_fusion), kind=kLoop, calls=%fused_computation.9 | loop fusion | flops 4718592 | bytes 3171840 | tf_op jit(solution)/shard_map/convert_element_type | solution.py:71
  133.0 1.3 collective-permute-start.1
  134.4 4.2 %collective-permute-start = (bf16[4,64,256]{2,1,0:T(8,128)(2,1)S(1)}, bf16[4,64,256]{2,1,0:T(8,128)(2,1)S(1)}, u32[]{:S(2)}, u32[]{:S(2)}) collective-permute-start(bf16[4,64,256]{2,1,0:T(8,128)(2,1)S(1)} %bitcast.108), channel_id=1, source_target_pairs={{0,8},{8,16},{16,24},{24,32},{32,40},{40,48},{48,56},{56,64},{64,7... | collective-permute-start | bytes 393224 | tf_op jit(solution)/shard_map/ppermute | solution.py:58
  138.6 1.6 convolution_convert_fusion
  141.3 11.9 %collective-permute-done.1 = bf16[4,64,256]{2,1,0:T(8,128)(2,1)S(1)} collective-permute-done((bf16[4,64,256]{2,1,0:T(8,128)(2,1)S(1)}, bf16[4,64,256]{2,1,0:T(8,128)(2,1)S(1)}, u32[]{:S(2)}, u32[]{:S(2)}) %collective-permute-start.1) | collective-permute-done | bytes 131104 | tf_op jit(solution)/shard_map/ppermute | solution.py:61
  153.9 1.3 fusion.38
  155.3 3.2 %reshape.221 = bf16[6,8,64,2,64]{4,3,2,1,0:T(2,128)(2,1)S(1)} reshape(bf16[6,8,64,128]{3,2,1,0:T(8,128)(2,1)} %get-tuple-element.8) | data formatting | bytes 1572864 | tf_op jit(solution)/shard_map/reshape | solution.py:128
  158.5 1.6 copy.106
  160.0 1.6 reshape.219
  162.3 1.3 copy-done.1
  163.6 2.4 %fusion.36 = (f32[6,2,64]{2,1,0:T(2,128)S(1)}, f32[6,2,64,8,64]{2,4,3,1,0:T(8,128)}) fusion(f32[6,2,8,64,64]{3,4,2,1,0:T(8,128)S(1)} %copy-done.1, pred[64,64]{0,1:T(8,128)(4,1)S(1)} %fusion.28, f32[6,2,64,512]{2,3,1,0:S(1)} %fusion.19), kind=kLoop, calls=%fused_computation.86 | loop fusion | flops 1572096 | bytes 4725760 | tf_op jit(solution)/shard_map/reduce_max | solution.py:154
  166.0 4.8 %all-to-all-done.1 = bf16[32,16,256]{2,1,0:T(8,128)(2,1)S(1)} async-done(((bf16[32,16,256]{2,1,0:T(8,128)(2,1)}), bf16[32,16,256]{2,1,0:T(8,128)(2,1)S(1)}, u32[]{:S(2)}, u32[]{:S(2)}) %all-to-all-start.1) | async-done | bytes 262176 | tf_op jit(solution)/shard_map/all_to_all | solution.py:17
  171.6 1.3 copy-done.2
  176.9 1.0 broadcast_in_dim.18
  177.9 5.6 %all-to-all-start.2 = ((bf16[8,384,128]{1,2,0:T(8,128)(2,1)}), bf16[8,384,128]{1,2,0:T(8,128)(2,1)S(1)}, u32[]{:S(2)}, u32[]{:S(2)}) async-start(bf16[8,384,128]{1,2,0:T(8,128)(2,1)} %broadcast_in_dim.18), calls=%async_computation.2 | async-start | bytes 1572864 | tf_op jit(solution)/shard_map/all_to_all | solution.py:17
  183.5 12.2 %all-to-all-done.2 = bf16[8,384,128]{1,2,0:T(8,128)(2,1)S(1)} async-done(((bf16[8,384,128]{1,2,0:T(8,128)(2,1)}), bf16[8,384,128]{1,2,0:T(8,128)(2,1)S(1)}, u32[]{:S(2)}, u32[]{:S(2)}) %all-to-all-start.2) | async-done | bytes 786464 | tf_op jit(solution)/shard_map/all_to_all | solution.py:17
  195.6 2.0 %fusion.16 = bf16[384,256]{1,0:T(8,128)(2,1)} fusion(bf16[384,1024]{0,1:T(8,128)(2,1)S(1)} %bitcast.105, bf16[1024,256]{1,0:T(8,128)(2,1)S(1)} %copy-done, f32[256]{0:T(256)S(1)} %slice.99, bf16[384,2048]{1,0:T(8,128)(2,1)} %param.13, s32[]{:T(128)S(6)} %select_n.37), kind=kOutput, calls=%fused_computation.27 | convolution fusion | flops 201719808 | bytes 1704964 | tf_op jit(solution)/shard_map/dot_general | solution.py:167
  (81 shorter events, 15.4 us)
Async XLA Ops:
  0.0 195.6 %copy-start = (bf16[1024,256]{1,0:T(8,128)(2,1)S(1)}, bf16[1024,256]{1,0:T(8,128)(2,1)}, u32[]{:S(2)}) copy-start(bf16[1024,256]{1,0:T(8,128)(2,1)} %param.25) | copy-start | bytes 1572868
  4.2 87.9 %all-to-all-start = ((f32[32,1,1280]{2,1,0:T(1,128)}), f32[32,1,1280]{2,1,0:T(1,128)S(1)}, u32[]{:S(2)}, u32[]{:S(2)}) async-start(f32[32,1,1280]{2,1,0:T(1,128)} %broadcast_in_dim.14), calls=%async_computation | async-start | bytes 327680 | tf_op jit(solution)/shard_map/all_to_all | solution.py:17
  87.8 3.7 %copy-start.10 = (bf16[2048]{0:T(1024)(128)(2,1)S(1)}, bf16[2048]{0:T(1024)(128)(2,1)}, u32[]{:S(2)}) copy-start(bf16[2048]{0:T(1024)(128)(2,1)} %param.20) | copy-start | bytes 12292
  87.8 3.7 %copy-start.9 = (bf16[16,2048]{1,0:T(8,128)(2,1)S(1)}, bf16[16,2048]{1,0:T(8,128)(2,1)}, u32[]{:S(2)}) copy-start(bf16[16,2048]{1,0:T(8,128)(2,1)} %param.15) | copy-start | bytes 196612
  87.8 3.9 %copy-start.3 = (bf16[384,2048]{1,0:T(8,128)(2,1)S(1)}, bf16[384,2048]{1,0:T(8,128)(2,1)}, u32[]{:S(2)}) copy-start(bf16[384,2048]{1,0:T(8,128)(2,1)} %param.13) | copy-start | bytes 4718596
  91.5 15.2 %copy-start.6 = (bf16[2048,128]{1,0:T(8,128)(2,1)S(1)}, bf16[2048,128]{1,0:T(8,128)(2,1)}, u32[]{:S(2)}) copy-start(bf16[2048,128]{1,0:T(8,128)(2,1)} %param.23) | copy-start | bytes 1572868
  91.5 15.4 %copy-start.5 = (bf16[2048,128]{1,0:T(8,128)(2,1)S(1)}, bf16[2048,128]{1,0:T(8,128)(2,1)}, u32[]{:S(2)}) copy-start(bf16[2048,128]{1,0:T(8,128)(2,1)} %param.22) | copy-start | bytes 1572868
  107.9 63.0 %all-to-all-start.1 = ((bf16[32,16,256]{2,1,0:T(8,128)(2,1)}), bf16[32,16,256]{2,1,0:T(8,128)(2,1)S(1)}, u32[]{:S(2)}, u32[]{:S(2)}) async-start(bf16[32,16,256]{2,1,0:T(8,128)(2,1)} %broadcast_in_dim.17), calls=%async_computation.1 | async-start | bytes 524288 | tf_op jit(solution)/shard_map/all_to_all | solution.py:17
  133.0 20.2 %collective-permute-start.1 = (bf16[4,64,256]{2,1,0:T(8,128)(2,1)S(1)}, bf16[4,64,256]{2,1,0:T(8,128)(2,1)S(1)}, u32[]{:S(2)}, u32[]{:S(2)}) collective-permute-start(bf16[4,64,256]{2,1,0:T(8,128)(2,1)S(1)} %bitcast.107), channel_id=1, source_target_pairs={{8,0},{16,8},{24,16},{32,24},{40,32},{48,40},{56,48},{64,56},{72,6... | collective-permute-start | bytes 393224 | tf_op jit(solution)/shard_map/ppermute | solution.py:61
  134.4 18.8 %collective-permute-start = (bf16[4,64,256]{2,1,0:T(8,128)(2,1)S(1)}, bf16[4,64,256]{2,1,0:T(8,128)(2,1)S(1)}, u32[]{:S(2)}, u32[]{:S(2)}) collective-permute-start(bf16[4,64,256]{2,1,0:T(8,128)(2,1)S(1)} %bitcast.108), channel_id=1, source_target_pairs={{0,8},{8,16},{16,24},{24,32},{32,40},{40,48},{48,56},{56,64},{64,7... | collective-permute-start | bytes 393224 | tf_op jit(solution)/shard_map/ppermute | solution.py:58
  160.0 1.7 copy-start.4
  161.7 1.9 copy-start.1
  163.6 7.4 %copy-start.8 = (bf16[6,64,2,64]{3,1,0,2:T(8,128)(2,1)S(1)}, bf16[6,64,2,64]{3,1,0,2:T(8,128)(2,1)}, u32[]{:S(2)}) copy-start(bf16[6,64,2,64]{3,1,0,2:T(8,128)(2,1)} %copy.111) | copy-start | bytes 294916
  171.0 1.9 copy-start.2
  173.4 1.4 copy-start.7
  177.9 17.8 %all-to-all-start.2 = ((bf16[8,384,128]{1,2,0:T(8,128)(2,1)}), bf16[8,384,128]{1,2,0:T(8,128)(2,1)S(1)}, u32[]{:S(2)}, u32[]{:S(2)}) async-start(bf16[8,384,128]{1,2,0:T(8,128)(2,1)} %broadcast_in_dim.18), calls=%async_computation.2 | async-start | bytes 1572864 | tf_op jit(solution)/shard_map/all_to_all | solution.py:17
where the time goes:
time: 199 us; the launch traced here: 198 us
  starting transfers between devices  79.2 us (40%)
  local copies, waits for them, and re-layouts  57.2 us (29%)
  waiting for transfers between devices  28.9 us (15%)
  blocking collectives  14.3 us (7%)
  matrix products  10.4 us (5%)
  other arithmetic  7.22 us (4%)
    all_to_all x3, starting transfers between devices, from_everyone(): return lax.all_to_all(copies, axis, split_axis=0, concat_axis=0, tiled=True)  73.7 us
    gather x2, local copies, waits for them, and re-layouts, local(): table_cols = offset_bias[:, :, col_offset]  33.8 us
    all_to_all x3, waiting for transfers between devices, from_everyone(): return lax.all_to_all(copies, axis, split_axis=0, concat_axis=0, tiled=True)  17 us
    all_gather x1, blocking collectives, sent_together(): filled, at, done = (lax.all_gather(both, axis, axis=dim, tiled=True), 0, [])  14.3 us
    ppermute x1, waiting for transfers between devices, extended(): lax.ppermute(lax.slice_in_dim(block, 0, width, axis=dim), axis, backward)  11.9 us
    gather x2, local copies, waits for them, and re-layouts, local(): lax.dynamic_slice_in_dim(table_cols, offset_row, WIN_H, 1)  6.16 us
    reshape x2, local copies, waits for them, and re-layouts, local(): windows[..., :head_width]  4.78 us
    unnamed x25, local copies, waits for them, and re-layouts  4.53 us
  transfers between devices with their start and end apart: 5, of which 3 were waited for; matrix products, arithmetic and copies ran while one was open for 30% of the time, Pallas kernels for 0%

commit v1 on v0

v1 whole, which is shorter than its diff:
```python
import functools

import jax
import jax.numpy as jnp
from jax import lax
from jax.experimental import pallas as pl
from jax.experimental.pallas import tpu as pltpu
from jax.sharding import PartitionSpec as P

HEAD_DIM = 64
GRID_W = 64
WIN_H = 8
WIN_W = 16
EPSILON = 1e-06
LANES = 128
BEFORE = WIN_H // 2
AFTER = WIN_H - BEFORE - 1
MESH = pl.DeviceIdType.MESH
F32 = jnp.float32
BF16 = jnp.bfloat16
NT = (((1,), (1,)), ((), ()))


def silu(v):
    v = v.astype(F32)
    return v / (1.0 + jnp.exp(-v))


def row_scales(rows_ref, start, inv_ref, at, step):
    width = rows_ref.shape[1]
    total = jnp.zeros((step, LANES), F32)
    for b in range(width // LANES):
        v = rows_ref[pl.ds(start, step), b * LANES : (b + 1) * LANES].astype(F32)
        total = total + v * v
    mean = jnp.sum(total, axis=1, keepdims=True) * (1.0 / width)
    inv_ref[pl.ds(at, step), :] = jnp.broadcast_to(lax.rsqrt(mean + EPSILON), (step, LANES))


def kernel(
    S, T,
    cond_ref, vec_ref, ctx_in, wsh_ref, wsc_ref, wga_ref, gain_ref, offs_ref,
    x_hbm, wq_hbm, wk_hbm, wv_hbm, wo_hbm,
    out_ref,
    x, w, wo, wl, wc, hb, ha, ctx, parts, mods, gate, offs, table, inv, inv_c,
    shf, shb, q_s, k_ext, v_ext, kc_s, vc_s, att,
    load_sem, ready, part_send, part_recv, ctx_send, ctx_recv, fwd_send, fwd_recv,
    halo_send, halo_recv, hb_send, hb_recv, ha_send, ha_recv, mod_send, mod_recv, att_send, att_recv,
):
    z = lax.axis_index("sp")
    t = lax.axis_index("tp")
    tokens, width = x.shape
    rows_dev = tokens // GRID_W
    cols = wsh_ref.shape[1]
    halves = cols // LANES
    rows_ctx = ctx_in.shape[0]
    slab = pl.ds(pl.multiple_of(t * cols, cols), cols)
    n_b, n_a = hb.shape[0], ha.shape[0]

    def peer(k):
        return lax.rem(t + k, T)

    def remote(src, dst, send, recv, **where):
        return pltpu.make_async_remote_copy(
            src_ref=src, dst_ref=dst, send_sem=send, recv_sem=recv,
            device_id=where, device_id_type=MESH,
        )

    barrier = pltpu.get_barrier_semaphore()
    for k in range(1, T):
        pl.semaphore_signal(barrier, inc=1, device_id={"tp": peer(k)}, device_id_type=MESH)

    def say_here(i, _):
        pl.semaphore_signal(barrier, inc=1, device_id={"sp": i}, device_id_type=MESH)
        return 0

    lax.fori_loop(z + 1, S, say_here, 0)

    loads = [
        pltpu.make_async_copy(x_hbm, x, load_sem.at[0]),
        pltpu.make_async_copy(wq_hbm, w.at[:, 0:LANES], load_sem.at[1]),
        pltpu.make_async_copy(wk_hbm, w.at[:, LANES : 2 * LANES], load_sem.at[2]),
        pltpu.make_async_copy(wv_hbm, w.at[:, 2 * LANES : 3 * LANES], load_sem.at[3]),
        pltpu.make_async_copy(wo_hbm, wo, load_sem.at[4]),
    ]
    for load in loads:
        load.start()

    row = lax.broadcasted_iota(jnp.int32, (16, cond_ref.shape[1]), 0)
    acts = jnp.where(row == 0, silu(cond_ref[...]), silu(vec_ref[...])).astype(BF16)
    shift_p = jnp.dot(acts, wsh_ref[...], preferred_element_type=F32)
    scale_p = jnp.dot(acts, wsc_ref[...], preferred_element_type=F32)
    gate_p = jnp.dot(acts, wga_ref[...], preferred_element_type=F32)
    for h in range(halves):
        lanes = slice(h * LANES, (h + 1) * LANES)
        parts[z, 2 * h : 2 * h + 2, :] = shift_p[0:2, lanes]
        parts[z, 4 + 2 * h : 6 + 2 * h, :] = scale_p[0:2, lanes]
        parts[z, 8 + h : 9 + h, :] = gate_p[0:1, lanes]
    ctx[pl.ds(pl.multiple_of(z * rows_ctx, rows_ctx), rows_ctx), :] = ctx_in[...]

    pl.semaphore_wait(barrier, z + (T - 1))

    def part_copy(src, to):
        return remote(parts.at[src], parts.at[src], part_send.at[to], part_recv.at[src], sp=to)

    def ctx_block(src):
        return ctx.at[pl.ds(pl.multiple_of(src * rows_ctx, rows_ctx), rows_ctx), slab]

    def ctx_copy(to):
        return remote(ctx_in.at[:, slab], ctx_block(z), ctx_send.at[to], ctx_recv.at[z], sp=to)

    def ctx_arrival(src):
        return remote(ctx_in.at[:, slab], ctx_block(src), ctx_send.at[src], ctx_recv.at[src], sp=src)

    def send_down(i, _):
        pl.semaphore_signal(ready.at[z], inc=1, device_id={"sp": i}, device_id_type=MESH)
        part_copy(z, i).start()
        return 0

    lax.fori_loop(0, z, send_down, 0)

    def send_down_ctx(i, _):
        ctx_copy(i).start()
        return 0

    lax.fori_loop(0, z, send_down_ctx, 0)

    loads[0].wait()
    below = lax.rem(z + (S - 1), S)
    above = lax.rem(z + 1, S)
    to_below = remote(x.at[0:n_a, slab], ha.at[:, slab], halo_send.at[0], halo_recv.at[0], sp=below)
    to_above = remote(x.at[tokens - n_b : tokens, slab], hb.at[:, slab], halo_send.at[1], halo_recv.at[1], sp=above)

    @pl.when(z > 0)
    def _():
        to_below.start()

    zeros_offs = jnp.zeros(offs.shape, F32)
    offs[...] = zeros_offs
    n_off = offs_ref.shape[1]
    for hd in range(2):
        offs[hd, 0:n_off, 0 : offs_ref.shape[2]] = offs_ref[hd]
    qc = lax.broadcasted_iota(jnp.int32, (GRID_W, LANES), 0)
    kcol = lax.rem(lax.broadcasted_iota(jnp.int32, (GRID_W, LANES), 1), GRID_W)
    c0 = jnp.clip(qc - WIN_W // 2, 0, GRID_W - WIN_W)
    inside = (kcol >= c0) & (kcol < c0 + WIN_W)
    for hd in range(2):
        here = offs[hd, 0:16, :]
        first = pltpu.roll(here, LANES - (WIN_W - 1), 1)
        second = pltpu.roll(here, GRID_W - (WIN_W - 1), 1)
        for o in range(n_off - 1):
            line = first[o : o + 1, :] + second[o + 1 : o + 2, :]
            spread = pltpu.roll(jnp.broadcast_to(line, (GRID_W, LANES)), 0, 1, stride=1, stride_axis=0)
            table[o, hd * GRID_W : (hd + 1) * GRID_W, :] = jnp.where(inside, spread, -jnp.inf)

    step = GRID_W

    def own_scales(i, _):
        at = pl.multiple_of(i * step, step)
        row_scales(x, at, inv, pl.multiple_of(n_b + at, step), step)
        return 0

    lax.fori_loop(0, tokens // step, own_scales, 0)
    shf[...] = jnp.zeros(shf.shape, F32)

    @pl.when(z == 0)
    def _():
        hb[...] = jnp.zeros(hb.shape, BF16)

    @pl.when(z == S - 1)
    def _():
        ha[...] = jnp.zeros(ha.shape, BF16)

    def spread_rows(ref, send, recv):
        for k in range(1, T):
            p = peer(k)
            remote(ref.at[:, slab], ref.at[:, slab], send.at[p], recv.at[t], tp=p).start()

    at_a, at_b = min(2, S - 1), min(4, S - 1)

    def one_source(i, _):
        src = lax.rem(z + i, S)

        @pl.when(src > z)
        def _():
            pl.semaphore_wait(ready.at[src], 1)
            part_copy(z, src).start()
            ctx_copy(src).start()

        @pl.when((i == 1) & (z < S - 1))
        def _():
            to_above.start()

        ctx_arrival(src).wait_recv()
        for k in range(1, T):
            p = peer(k)
            remote(ctx_block(src), ctx_block(src), fwd_send.at[p], fwd_recv.at[t], tp=p).start()

        @pl.when((i == at_a) & (z < S - 1))
        def _():
            to_below.wait_recv()
            spread_rows(ha, ha_send, ha_recv)

        @pl.when((i == at_b) & (z > 0))
        def _():
            to_above.wait_recv()
            spread_rows(hb, hb_send, hb_recv)

        return 0

    mid = max(S // 2, at_b + 1)
    lax.fori_loop(1, mid, one_source, 0)

    def slab_of(p):
        return pl.ds(pl.multiple_of(p * cols, cols), cols)

    def await_rows(ref, send, recv):
        for k in range(1, T):
            p = peer(k)
            remote(ref.at[:, slab_of(p)], ref.at[:, slab_of(p)], send.at[p], recv.at[p], tp=p).wait_recv()

    @pl.when(z < S - 1)
    def _():
        await_rows(ha, ha_send, ha_recv)

    @pl.when(z > 0)
    def _():
        await_rows(hb, hb_send, hb_recv)

    def before_scales(i, _):
        at = pl.multiple_of(i * step, step)
        row_scales(hb, at, inv, at, step)
        return 0

    def after_scales(i, _):
        at = pl.multiple_of(i * step, step)
        row_scales(ha, at, inv, pl.multiple_of(n_b + tokens + at, step), step)
        return 0

    lax.fori_loop(0, n_b // step, before_scales, 0)
    lax.fori_loop(0, n_a // step, after_scales, 0)
    for load in loads[1:]:
        load.wait()

    if mid < S:
        lax.fori_loop(mid, S, one_source, 0)

    def await_part(i, _):
        src = lax.rem(z + i, S)
        part_copy(src, src).wait_recv()
        return 0

    lax.fori_loop(1, S, await_part, 0)
    total = parts[0]
    for s in range(1, S):
        total = total + parts[s]
    mods[t] = total[0:8, :]
    gate[...] = total[8 : 8 + halves, :]
    for k in range(1, T):
        p = peer(k)
        remote(mods.at[t], mods.at[t], mod_send.at[p], mod_recv.at[t], tp=p).start()

    most = ctx.shape[0] - rows_ctx
    for k in range(1, T):
        p = peer(k)
        some = ctx.at[0:most, slab_of(p)]
        remote(some, some, fwd_send.at[p], fwd_recv.at[p], tp=p).wait_recv()
    c_step = min(step, ctx.shape[0])

    def ctx_scales(i, _):
        at = pl.multiple_of(i * c_step, c_step)
        row_scales(ctx, at, inv_c, at, c_step)
        return 0

    lax.fori_loop(0, ctx.shape[0] // c_step, ctx_scales, 0)

    for k in range(1, T):
        p = peer(k)
        remote(mods.at[p], mods.at[p], mod_send.at[p], mod_recv.at[p], tp=p).wait_recv()

    factors = []
    for h in range(halves):
        g = gain_ref[h].astype(F32)
        for m in range(2):
            factors.append((1.0 + mods[:, 4 + 2 * h + m, :]) * g)
    upright = jnp.concatenate(factors, axis=0).T
    for f in range(T):
        for h in range(halves):
            lo = (f * halves + h) * LANES
            block = w[lo : lo + LANES, :].astype(F32)
            at = 2 * h * T + f
            wl[lo : lo + LANES, :] = (block * upright[:, at : at + 1]).astype(BF16)
            at = (2 * h + 1) * T + f
            wc[lo : lo + LANES, :] = (block[:, LANES:] * upright[:, at : at + 1]).astype(BF16)
            shf[0:2, lo : lo + LANES] = mods[f, 2 * h : 2 * h + 2, :]
    shift = shf[...]
    high = shift.astype(BF16)
    shb[0:8, :] = high
    shb[8:16, :] = (shift - high.astype(F32)).astype(BF16)
    base = jnp.dot(shb[...], w[...], preferred_element_type=F32)
    base_l = base[0:1, :] + base[8:9, :]
    base_c = base[1:2, LANES:] + base[9:10, LANES:]

    def three(v):
        return jnp.concatenate([v, v, v], axis=1)

    def two(v):
        return jnp.concatenate([v, v], axis=1)

    own = jnp.dot(x[...], wl[...], preferred_element_type=F32)
    own = own * three(inv[n_b : n_b + tokens, :]) + base_l
    q_s[...] = (own[:, 0:LANES].astype(BF16).astype(F32) * HEAD_DIM ** (-0.5)).astype(BF16)
    k_ext[BEFORE : BEFORE + rows_dev] = own[:, LANES : 2 * LANES].astype(BF16).reshape(rows_dev, GRID_W, LANES)
    v_ext[BEFORE : BEFORE + rows_dev] = own[:, 2 * LANES :].astype(BF16).reshape(rows_dev, GRID_W, LANES)
    kv_b = jnp.dot(hb[...], wl[:, LANES:], preferred_element_type=F32) * two(inv[0:n_b, :]) + base_l[:, LANES:]
    k_ext[0:BEFORE] = kv_b[:, 0:LANES].astype(BF16).reshape(BEFORE, GRID_W, LANES)
    v_ext[0:BEFORE] = kv_b[:, LANES:].astype(BF16).reshape(BEFORE, GRID_W, LANES)
    kv_a = jnp.dot(ha[...], wl[:, LANES:], preferred_element_type=F32) * two(inv[n_b + tokens :, :]) + base_l[:, LANES:]
    k_ext[BEFORE + rows_dev :] = kv_a[:, 0:LANES].astype(BF16).reshape(AFTER, GRID_W, LANES)
    v_ext[BEFORE + rows_dev :] = kv_a[:, LANES:].astype(BF16).reshape(AFTER, GRID_W, LANES)
    kv_c = jnp.dot(ctx[...], wc[...], preferred_element_type=F32) * two(inv_c[...]) + base_c
    kc_s[...] = kv_c[:, 0:LANES].astype(BF16)
    vc_s[...] = kv_c[:, LANES:].astype(BF16)

    head0 = lax.broadcasted_iota(jnp.int32, (GRID_W, LANES), 1) < HEAD_DIM
    own_cols = pl.ds(pl.multiple_of(t * LANES, LANES), LANES)
    group = 2
    for r in range(rows_dev):
        grid_row = z * rows_dev + r
        first_row = jnp.clip(grid_row - WIN_H // 2, 0, S * rows_dev - WIN_H)
        start = first_row - z * rows_dev + BEFORE
        offset = first_row - grid_row + WIN_H - 1
        q = q_s[r * GRID_W : (r + 1) * GRID_W, :]
        none = jnp.zeros_like(q)
        q2 = jnp.concatenate([jnp.where(head0, q, none), jnp.where(head0, none, q)], axis=0)
        keys = k_ext[pl.ds(start, WIN_H)].reshape(WIN_H * GRID_W, LANES)
        values = v_ext[pl.ds(start, WIN_H)].reshape(WIN_H * GRID_W, LANES)
        s_win = lax.dot_general(q2, keys, NT, preferred_element_type=F32)
        s_win = s_win + jnp.concatenate([table[offset + 2 * j] for j in range(WIN_H // 2)], axis=1)
        s_ctx = lax.dot_general(q2, kc_s[...], NT, preferred_element_type=F32)
        top = jnp.maximum(jnp.max(s_win, axis=1, keepdims=True), jnp.max(s_ctx, axis=1, keepdims=True))
        e_win = jnp.exp(s_win - top)
        e_ctx = jnp.exp(s_ctx - top)
        norm = jnp.sum(e_win, axis=1, keepdims=True) + jnp.sum(e_ctx, axis=1, keepdims=True)
        o = jnp.dot(e_win.astype(BF16), values, preferred_element_type=F32)
        o = o + jnp.dot(e_ctx.astype(BF16), vc_s[...], preferred_element_type=F32)
        o = o / norm
        o = jnp.where(head0, o[0:GRID_W, :], o[GRID_W:, :])
        att[r * GRID_W : (r + 1) * GRID_W, own_cols] = o.astype(BF16)
        if r % group == group - 1:
            g = r // group
            rows = slice(g * group * GRID_W, (g + 1) * group * GRID_W)
            for k in range(1, T):
                p = peer(k)
                remote(att.at[rows, own_cols], att.at[rows, own_cols], att_send.at[p, g], att_recv.at[t, g], tp=p).start()

    for g in range(rows_dev // group):
        rows = slice(g * group * GRID_W, (g + 1) * group * GRID_W)
        for k in range(1, T):
            p = peer(k)
            theirs = pl.ds(pl.multiple_of(p * LANES, LANES), LANES)
            remote(att.at[rows, theirs], att.at[rows, theirs], att_send.at[p, g], att_recv.at[p, g], tp=p).wait_recv()
        branch = jnp.dot(att[rows, :], wo[...], preferred_element_type=F32)
        residual = x[rows, slab].astype(F32)
        for h in range(halves):
            lanes = slice(h * LANES, (h + 1) * LANES)
            out_ref[rows, lanes] = (residual[:, lanes] + gate[h : h + 1, :] * branch[:, lanes]).astype(BF16)

    def sent_parts(i, _):
        to = lax.rem(z + i, S)
        part_copy(z, to).wait_send()
        ctx_copy(to).wait_send()
        return 0

    lax.fori_loop(1, S, sent_parts, 0)

    @pl.when(z > 0)
    def _():
        to_below.wait_send()
        for k in range(1, T):
            p = peer(k)
            remote(hb.at[:, slab], hb.at[:, slab], hb_send.at[p], hb_recv.at[t], tp=p).wait_send()

    @pl.when(z < S - 1)
    def _():
        to_above.wait_send()
        for k in range(1, T):
            p = peer(k)
            remote(ha.at[:, slab], ha.at[:, slab], ha_send.at[p], ha_recv.at[t], tp=p).wait_send()

    for k in range(1, T):
        p = peer(k)
        some = ctx.at[0:most, slab]
        remote(some, some, fwd_send.at[p], fwd_recv.at[t], tp=p).wait_send()
        remote(mods.at[t], mods.at[t], mod_send.at[p], mod_recv.at[t], tp=p).wait_send()
        for g in range(rows_dev // group):
            rows = slice(g * group * GRID_W, (g + 1) * group * GRID_W)
            remote(att.at[rows, own_cols], att.at[rows, own_cols], att_send.at[p, g], att_recv.at[t, g], tp=p).wait_send()


def local(
    S, T, latent, conditioning, context, ctx_vector, w_shift, w_scale, w_gate, norm_gain,
    w_query, w_key, w_value, offset_bias, w_out,
):
    tokens, width = latent.shape
    cols = w_shift.shape[1]
    halves = cols // LANES
    rows_dev = tokens // GRID_W
    n_ctx = context.shape[0] * S
    ext = rows_dev + BEFORE + AFTER
    heads, n_off, _ = offset_bias.shape
    dma = pltpu.SemaphoreType.DMA
    vmem = pl.BlockSpec(memory_space=pltpu.VMEM)
    hbm = pl.BlockSpec(memory_space=pltpu.HBM)
    gain = norm_gain.reshape(T, halves, LANES).transpose(1, 0, 2)
    return pl.pallas_call(
        functools.partial(kernel, S, T),
        name="modulated_attention",
        out_shape=jax.ShapeDtypeStruct((tokens, cols), BF16),
        in_specs=[vmem] * 8 + [hbm] * 5,
        out_specs=vmem,
        scratch_shapes=[
            pltpu.VMEM((tokens, width), BF16),
            pltpu.VMEM((width, 3 * LANES), BF16),
            pltpu.VMEM(w_out.shape, BF16),
            pltpu.VMEM((width, 3 * LANES), BF16),
            pltpu.VMEM((width, 2 * LANES), BF16),
            pltpu.VMEM((BEFORE * GRID_W, width), BF16),
            pltpu.VMEM((AFTER * GRID_W, width), BF16),
            pltpu.VMEM((n_ctx, width), BF16),
            pltpu.VMEM((S, 8 + halves, LANES), F32),
            pltpu.VMEM((T, 8, LANES), F32),
            pltpu.VMEM((halves, LANES), F32),
            pltpu.VMEM((heads, 16, LANES), F32),
            pltpu.VMEM((n_off - 1, heads * GRID_W, LANES), F32),
            pltpu.VMEM((ext * GRID_W, LANES), F32),
            pltpu.VMEM((n_ctx, LANES), F32),
            pltpu.VMEM((8, width), F32),
            pltpu.VMEM((16, width), BF16),
            pltpu.VMEM((tokens, LANES), BF16),
            pltpu.VMEM((ext, GRID_W, LANES), BF16),
            pltpu.VMEM((ext, GRID_W, LANES), BF16),
            pltpu.VMEM((n_ctx, LANES), BF16),
            pltpu.VMEM((n_ctx, LANES), BF16),
            pltpu.VMEM((tokens, T * LANES), BF16),
            dma((5,)),
            pltpu.SemaphoreType.REGULAR((S,)),
            dma((S,)), dma((S,)), dma((S,)), dma((S,)),
            dma((T,)), dma((T,)),
            dma((2,)), dma((2,)),
            dma((T,)), dma((T,)), dma((T,)), dma((T,)),
            dma((T,)), dma((T,)),
            dma((T, rows_dev // 2)), dma((T, rows_dev // 2)),
        ],
        compiler_params=pltpu.CompilerParams(collective_id=0, has_side_effects=True),
    )(
        conditioning.reshape(1, -1), ctx_vector.reshape(1, -1), context, w_shift, w_scale, w_gate,
        gain, offset_bias, latent, w_query, w_key, w_value, w_out,
    )


def solution(mesh):
    return jax.shard_map(
        functools.partial(local, mesh.shape["sp"], mesh.shape["tp"]),
        mesh=mesh,
        in_specs=(
            P(("grp", "sp"), None),
            P(("grp", "sp")),
            P(("grp", "sp"), None),
            P("sp"),
            P("sp", "tp"),
            P("sp", "tp"),
            P("sp", "tp"),
            P(),
            P(None, "tp"),
            P(None, "tp"),
            P(None, "tp"),
            P("tp", None, None),
            P(None, "tp"),
        ),
        out_specs=P(("grp", "sp"), "tp"),
        check_vma=False,
    )
```

time: 199 us -> 129 us (0.65)
  the two profiles are of different devices: /device:TPU:33 before, /device:TPU:1957 now
where the time goes in v1:
time: 129 us
  Pallas kernels  124 us (96%)
  local copies, waits for them, and re-layouts  4.21 us (3%)
    pallas_call x1, Pallas kernels, local(): pl.pallas_call(functools.partial(kernel, S, T), name='modulated_attention...  124 us
    unnamed x2, local copies, waits for them, and re-layouts  2.94 us

profile of v1, /device:TPU:1957, one launch (start us, length us, event | category | flops | bytes accessed | tf_op | source)
XLA Modules:
  0.0 128.7 jit_solution(14602991339893115344)
XLA Ops:
  0.0 1.3 copy.18
  1.3 1.3 %copy.16.offs_ref = f32[2,15,31]{2,1,0:T(8,128)} copy(f32[2,15,31]{2,0,1:T(2,128)} %param.24) | data formatting | bytes 7440 | tf_op args[11]
  2.6 124.5 %modulated_attention.1 = bf16[384,256]{1,0:T(8,128)(2,1)} custom-call(bf16[1,64]{1,0:T(2,128)(2,1)} %bitcast.8, bf16[1,64]{1,0:T(2,128)(2,1)} %bitcast.9, bf16[16,2048]{1,0:T(8,128)(2,1)} %ctx_in.1, bf16[64,256]{1,0:T(8,128)(2,1)} %wsh_ref.1, bf16[64,256]{1,0:T(8,128)(2,1)} %wsc_ref.1, bf16[64,256]{1,0:T(8,128)(2,1)} %wga_ref.1, bf16[2,8,128]{2,1,0:T(8,128)(2,1)} %bitcast.6, ...), custom_call_target="tpu_custom_call" | custom-call | tf_op jit(solution)/shard_map/modulated_attention/pallas_call | solution.py:415
  127.1 1.6 %copy.20 = bf16[384,256]{1,0:T(8,128)(2,1)} copy(bf16[384,256]{1,0:T(8,128)(2,1)} %modulated_attention.1) | data formatting | bytes 393216
